TPU v7x, 32 devices: a whole 2x2x4 slice. The times are simulated.
32 devices in a mesh: sp: 4 (over z), dp: 8 (over y, x, core).
Axes of the slice: x: 2, y: 2, z: 4, core: 2. Of those that a mesh axis runs over, the one named last changes fastest.
Arguments:
- probe_vectors: bfloat16 [4096, 1024], P(('dp', 'sp')), may hold values from -6 to 6
- address_vectors: bfloat16 [4096, 1024], P(('dp', 'sp')), may hold values from -6 to 6
- content_vectors: bfloat16 [4096, 2048], P(('dp', 'sp')), may hold values from -6 to 6
- adjoint_of_result: bfloat16 [4096, 2048], P(('dp', 'sp')), may hold values from -0.5 to 0.5
- compact_factor: bfloat16 [4096, 64], P(('dp', 'sp')), may hold values from -7.5 to 7.5
- latent_to_damping_map: bfloat16 [64, 1024], replicated, may hold values from -0.75 to 0.75
- damping_shift_term: float32 [1024], replicated
- surplus_damping: bfloat16 [4096, 16], P(('dp', 'sp')), may hold values from -0.7 to 0
Outputs:
- query_grad: bfloat16 [4096, 1024], P(('dp', 'sp'))
- key_grad: bfloat16 [4096, 1024], P(('dp', 'sp'))
- value_grad: bfloat16 [4096, 2048], P(('dp', 'sp'))
- latent_grad: bfloat16 [4096, 64], P(('dp', 'sp'))
- weight_grad: float32 [64, 1024], replicated
All inputs are finite; a program needn't handle non-finite values.
Results may differ from a plain program's by a relative error of at most 0.005.
Values may be sent and summed in bfloat16 or wider, within the bound.
No kernel may reach another device: no remote copies, remote signals or barrier semaphores. Data moves between devices by JAX's collectives and lax.ppermute only.
A program may use at most 64 MiB of HBM per device.

v0:
```python
import jax
import jax.numpy as jnp
from jax import lax
from jax.sharding import PartitionSpec as P

KEY_CHANNELS = 64
VALUE_DIM = 128
BLOCK = 64
gate_norm = 16.0
highest = lax.Precision.HIGHEST


def carry_states(block_total, increments):
    log_totals = block_total[:, :, 0, :]
    running = jnp.cumsum(log_totals, axis=1)
    before = running - log_totals
    blocks = log_totals.shape[1]
    order = jnp.arange(blocks, dtype=jnp.int32)
    earlier_mask = (order[None, :] < order[:, None])[None, :, :, None]
    exponent = before[:, :, None, :] - running[:, None, :, :]
    exponent = jnp.where(earlier_mask, exponent, jnp.zeros_like(exponent))
    weights = jnp.where(earlier_mask, jnp.exp(exponent), jnp.zeros_like(exponent))
    return jnp.einsum("hnmk,mhkv->nhkv", weights, increments, precision=highest)


def gla_forward(probe_vectors, address_vectors, content_vectors, logarithm_decay):
    head_count, seq_len, key_width = probe_vectors.shape
    value_width = content_vectors.shape[2]
    blocks = seq_len // BLOCK

    def blocked(tensor):
        return tensor.reshape(head_count, blocks, BLOCK, tensor.shape[2])

    cumulative = jnp.cumsum(blocked(logarithm_decay), axis=2)
    block_total = cumulative[:, :, BLOCK - 1 :, :]
    keys_block = blocked(address_vectors)
    query_decayed = blocked(probe_vectors) * key_width ** (-0.5) * jnp.exp(cumulative)
    key_inverse = keys_block * jnp.exp(-cumulative)
    key_to_end = keys_block * jnp.exp(block_total - cumulative)
    value_block = blocked(content_vectors)
    scores = jnp.einsum("hnik,hnjk->hnij", query_decayed, key_inverse, precision=highest)
    positions = jnp.arange(BLOCK, dtype=jnp.int32)
    causal = positions[:, None] >= positions[None, :]
    scores = jnp.where(causal, scores, jnp.zeros_like(scores))
    within_block = jnp.einsum("hnij,hnjv->hniv", scores, value_block, precision=highest)
    increments = jnp.einsum("hnjk,hnjv->nhkv", key_to_end, value_block, precision=highest)
    earlier = carry_states(block_total, increments)
    carried = jnp.einsum("hnik,nhkv->hniv", query_decayed, earlier, precision=highest)
    return (within_block + carried).reshape(head_count, seq_len, value_width)


def split_into_heads(tensor, width):
    return tensor.astype(jnp.float32).reshape(tensor.shape[0], -1, width).transpose(1, 0, 2)


def to_rows(tensor):
    return tensor.transpose(1, 0, 2).reshape(tensor.shape[1], tensor.shape[0] * tensor.shape[2])


def on_device(
    probe_vectors,
    address_vectors,
    content_vectors,
    adjoint_of_result,
    compact_factor,
    latent_to_damping_map,
    damping_shift_term,
    surplus_damping,
):
    query_per_head, key_per_head, value_per_head, upstream_heads, spike_heads = (
        lax.all_to_all(probe_vectors, "sp", split_axis=1, concat_axis=0, tiled=True),
        lax.all_to_all(address_vectors, "sp", split_axis=1, concat_axis=0, tiled=True),
        lax.all_to_all(content_vectors, "sp", split_axis=1, concat_axis=0, tiled=True),
        lax.all_to_all(adjoint_of_result, "sp", split_axis=1, concat_axis=0, tiled=True),
        lax.all_to_all(surplus_damping, "sp", split_axis=1, concat_axis=0, tiled=True),
    )
    local_width = query_per_head.shape[1]
    hidden_code_rows = lax.all_gather(compact_factor, "sp", axis=0, tiled=True)
    column_start = lax.axis_index("sp") * local_width
    weight_local = lax.dynamic_slice_in_dim(latent_to_damping_map, column_start, local_width, 1)
    bias_local = lax.dynamic_slice_in_dim(damping_shift_term, column_start, local_width, 0)
    gate_logit = (
        jnp.dot(hidden_code_rows, weight_local, preferred_element_type=jnp.float32) + bias_local
    )
    forget_rate_rows = jax.nn.log_sigmoid(gate_logit) / gate_norm
    logarithm_decay = (
        split_into_heads(forget_rate_rows, KEY_CHANNELS)
        + spike_heads.astype(jnp.float32).T[:, :, None]
    )
    _, pullback = jax.vjp(
        gla_forward,
        split_into_heads(query_per_head, KEY_CHANNELS),
        split_into_heads(key_per_head, KEY_CHANNELS),
        split_into_heads(value_per_head, VALUE_DIM),
        logarithm_decay,
    )
    grad_query, grad_key, grad_value, grad_decay = pullback(
        split_into_heads(upstream_heads, VALUE_DIM)
    )
    query_grad, key_grad, value_grad = (
        lax.all_to_all(
            to_rows(grad_query).astype(jnp.bfloat16), "sp", split_axis=0, concat_axis=1, tiled=True
        ),
        lax.all_to_all(
            to_rows(grad_key).astype(jnp.bfloat16), "sp", split_axis=0, concat_axis=1, tiled=True
        ),
        lax.all_to_all(
            to_rows(grad_value).astype(jnp.bfloat16), "sp", split_axis=0, concat_axis=1, tiled=True
        ),
    )
    decay_rows = to_rows(grad_decay)
    gate_grad = (decay_rows * jax.nn.sigmoid(-gate_logit) / gate_norm).astype(jnp.bfloat16)
    partial_latent = jnp.einsum(
        "sc,rc->sr", gate_grad, weight_local, preferred_element_type=jnp.float32
    )
    latent_grad = lax.psum_scatter(partial_latent, "sp", scatter_dimension=0, tiled=True).astype(
        jnp.bfloat16
    )
    local_weight = jnp.einsum(
        "sr,sc->rc", hidden_code_rows, gate_grad, preferred_element_type=jnp.float32
    )
    summed = lax.psum(local_weight, "dp")
    weight_grad = lax.all_gather(summed, "sp", axis=1, tiled=True)
    return (query_grad, key_grad, value_grad, latent_grad, weight_grad)


def solution(mesh):
    return jax.shard_map(
        on_device,
        mesh=mesh,
        in_specs=(
            P(("dp", "sp"), None),
            P(("dp", "sp"), None),
            P(("dp", "sp"), None),
            P(("dp", "sp"), None),
            P(("dp", "sp"), None),
            P(),
            P(),
            P(("dp", "sp"), None),
        ),
        out_specs=(
            P(("dp", "sp"), None),
            P(("dp", "sp"), None),
            P(("dp", "sp"), None),
            P(("dp", "sp"), None),
            P(),
        ),
        check_vma=False,
    )
```

profile of v0, /device:TPU:0, one launch (start us, length us, event | category | flops | bytes accessed | tf_op | source)
XLA Modules:
  0.0 277.0 jit_solution(3052615414394250195)
XLA Ops:
  8.0 6.5 %all-to-all-start.1 = ((bf16[128,4,4]{0,2,1:T(4,128)(2,1)}), bf16[128,4,4]{0,2,1:T(4,128)(2,1)S(1)}, u32[]{:S(2)}, u32[]{:S(2)}) async-start(bf16[128,4,4]{0,2,1:T(4,128)(2,1)} %bitcast.169), calls=%async_computation.1 | async-start | bytes 8192 | tf_op jit(solution)/shard_map/all_to_all | solution.py:75
  14.5 1.8 copy.214
  16.3 3.8 %all-to-all-done.1 = bf16[128,4,4]{0,2,1:T(4,128)(2,1)S(1)} async-done(((bf16[128,4,4]{0,2,1:T(4,128)(2,1)}), bf16[128,4,4]{0,2,1:T(4,128)(2,1)S(1)}, u32[]{:S(2)}, u32[]{:S(2)}) %all-to-all-start.1) | async-done | bytes 4128 | tf_op jit(solution)/shard_map/all_to_all | solution.py:75
  20.1 3.5 %all-to-all-start.5 = ((bf16[128,4,256]{0,2,1:T(8,128)(2,1)}), bf16[128,4,256]{0,2,1:T(8,128)(2,1)S(1)}, u32[]{:S(2)}, u32[]{:S(2)}) async-start(bf16[128,4,256]{0,2,1:T(8,128)(2,1)} %bitcast.24), calls=%async_computation.5 | async-start | bytes 524288 | tf_op jit(solution)/shard_map/all_to_all | solution.py:71
  24.5 7.0 %all-to-all-done.5 = bf16[128,4,256]{0,2,1:T(8,128)(2,1)S(1)} async-done(((bf16[128,4,256]{0,2,1:T(8,128)(2,1)}), bf16[128,4,256]{0,2,1:T(8,128)(2,1)S(1)}, u32[]{:S(2)}, u32[]{:S(2)}) %all-to-all-start.5) | async-done | bytes 262176 | tf_op jit(solution)/shard_map/all_to_all | solution.py:71
  31.5 3.4 %all-to-all-start = ((bf16[128,4,256]{0,2,1:T(8,128)(2,1)}), bf16[128,4,256]{0,2,1:T(8,128)(2,1)S(1)}, u32[]{:S(2)}, u32[]{:S(2)}) async-start(bf16[128,4,256]{0,2,1:T(8,128)(2,1)} %bitcast), calls=%async_computation | async-start | bytes 524288 | tf_op jit(solution)/shard_map/all_to_all | solution.py:72
  36.6 12.5 %all_gather.6 = bf16[512,64]{0,1:T(8,128)(2,1)S(1)} all-gather(bf16[128,64]{0,1:T(8,128)(2,1)S(1)} %copy-done.31), channel_id=1, replica_groups=mesh['sp'=4,'dp'=8] {'sp'}, dimensions={0}, use_global_device_ids=true | all-gather | bytes 81920 | tf_op jit(solution)/shard_map/all_gather | solution.py:78
  51.7 4.1 %all-to-all-start.3 = ((bf16[128,4,512]{2,0,1:T(8,128)(2,1)}), bf16[128,4,512]{2,0,1:T(8,128)(2,1)}, u32[]{:S(2)}, u32[]{:S(2)}) async-start(bf16[128,4,512]{2,0,1:T(8,128)(2,1)} %bitcast.143), calls=%async_computation.3 | async-start | bytes 1048576 | tf_op jit(solution)/shard_map/all_to_all | solution.py:74
  58.0 25.9 %fusion.46 = f32[4,8,64,64]{3,1,2,0:T(8,128)S(1)} fusion(f32[4,8,64,64]{3,1,2,0:T(8,128)S(1)} %copy.194), kind=kOutput, calls=%fused_computation.84 | output fusion | flops 8257536 | bytes 1048576 | tf_op jit(solution)/shard_map/jvp(jit(cumsum))/reduce_window_sum | solution.py:34
  83.9 5.1 %all-to-all-start.2 = ((bf16[128,4,512]{2,0,1:T(8,128)(2,1)}), bf16[128,4,512]{2,0,1:T(8,128)(2,1)}, u32[]{:S(2)}, u32[]{:S(2)}) async-start(bf16[128,4,512]{2,0,1:T(8,128)(2,1)} %bitcast.144), calls=%async_computation.2 | async-start | bytes 1048576 | tf_op jit(solution)/shard_map/all_to_all | solution.py:73
  95.1 2.0 reshape.161
  97.0 1.9 copy.205
  99.4 2.0 reshape.159
  103.7 2.9 %convolution_bitcast_fusion = f32[8,4,64,128]{3,0,2,1:T(8,128)S(1)} fusion(f32[4,64,128,8]{2,1,3,0:T(8,128)S(1)} %convolution_bitcast_fusion.3, f32[4,8,64]{1,2,0:T(8,128)S(1)} %copy-done.23, f32[4,8,64]{1,2,0:T(8,128)S(1)} %copy-done.24, pred[8,8]{1,0:T(8,128)(4,1)S(1)} %copy-done.32), kind=kOutput, calls=%fused_computation.4 | convolution fusion | flops 25214976 | bytes 2113600 | tf_op jit(solution)/shard_map/transpose(jvp(hnmk,mhkv->nhkv))/dot_general | solution.py:23
  106.6 2.8 %fusion.18 = (f32[4,8,64]{2,1,0:T(8,128)}, f32[4,8,64,64]{2,3,1,0:T(8,128)S(1)}, f32[4,8,64,64]{2,3,1,0:T(8,128)}) fusion(f32[4,8,64,64]{2,3,1,0:T(8,128)S(1)} %copy.195, f32[4,8,64,64]{2,1,3,0:T(8,128)S(1)} %reshape.166, f32[4,8,64]{2,1,0:T(8,128)S(1)} %slice_bitcast_fusion, bf16[4,8,64,128]{3,2,1,0:T(8,128)(2,1)S(1)} %bitcast.150, ...), kind=kOutput, calls=%fused_computation.40 | convolution fusion | flops 201979904 | bytes 3686400 | tf_op jit(solution)/shard_map/transpose(jvp(hnjk,hnjv->nhkv))/dot_general | solution.py:46
  110.4 2.5 convolution_bitcast_fusion.1
  112.9 4.3 %fusion.45 = (f32[4,8,64]{1,2,0:T(8,128)}, f32[4,8,64]{1,2,0:T(8,128)}) fusion(f32[4,8,64]{1,2,0:T(8,128)S(1)} %copy-done.23, f32[4,8,64]{1,2,0:T(8,128)S(1)} %copy-done.24, f32[8,4,64,128]{3,2,1,0:T(8,128)S(1)} %fusion.6, f32[4,64,128,8]{2,1,3,0:T(8,128)S(1)} %convolution_bitcast_fusion.3, pred[8,8]{1,0:T(8,128)(4,1)S(1)} %copy-done.32), kind=kOutput, calls=%fused_computation.83 | convolution fusion | flops 25276416 | bytes 2129984 | tf_op jit(solution)/shard_map/transpose(jvp(hnmk,mhkv->nhkv))/dot_general | solution.py:23
  117.3 2.0 convolution_bitcast_fusion.4
  122.2 1.4 copy.244
  123.6 1.4 copy.245
  125.1 1.6 convolution_select_fusion
  128.6 1.5 fusion.3
  130.1 3.7 %pad_add_fusion = (f32[4,8,64,64]{2,3,1,0:T(8,128)}, bf16[4,8,64,64]{2,3,1,0:T(8,128)(2,1)}, bf16[4,8,64,64]{2,3,1,0:T(8,128)(2,1)S(1)}) fusion(f32[4,8,1,64]{2,3,1,0:T(8,128)S(1)} %fusion.3, f32[4,8,64,64]{2,3,1,0:T(8,128)S(1)} %fusion.44, f32[4,8,64,64]{2,1,3,0:T(8,128)S(1)} %mul.72, f32[4,8,64,64]{2,3,1,0:T(8,128)S(1)} %copy.195, ...), kind=kOutput, calls=%fused_computation.22 | convolution fusion | flops 103677952 | bytes 4734976 | tf_op jit(solution)/shard_map/transpose(jvp(hnik,hnjk->hnij))/dot_general | solution.py:41
  137.1 1.7 copy.213
  138.8 4.8 %all-to-all-start.4 = ((bf16[4,128,256]{1,2,0:T(8,128)(2,1)}), bf16[4,128,256]{1,2,0:T(8,128)(2,1)S(1)}, u32[]{:S(2)}, u32[]{:S(2)}) async-start(bf16[4,128,256]{1,2,0:T(8,128)(2,1)} %copy.213), calls=%async_computation.4 | async-start | bytes 524288 | tf_op jit(solution)/shard_map/all_to_all | solution.py:101
  143.6 3.1 %convolution_select_fusion.2 = f32[4,8,64,64]{3,2,1,0:T(8,128)} fusion(pred[64,64]{1,0:T(8,128)(4,1)S(1)} %copy-done.28, f32[4,8,64,64]{2,1,3,0:T(8,128)S(1)} %reshape.166, f32[4,8,64,64]{2,3,1,0:T(8,128)S(1)} %copy.195, f32[4,8,64,64]{2,1,3,0:T(8,128)S(1)} %mul.72), kind=kOutput, calls=%fused_computation.11 | convolution fusion | flops 101187584 | bytes 2101248 | tf_op jit(solution)/shard_map/jvp(hnik,hnjk->hnij)/dot_general | solution.py:41
  148.3 3.2 %fusion.11 = f32[4,8,64,128]{3,2,1,0:T(8,128)S(1)} fusion(f32[4,8,64,64]{2,3,1,0:T(8,128)S(1)} %copy-done.4, f32[8,4,64,128]{3,0,2,1:T(8,128)} %copy-done.9), kind=kOutput, calls=%fused_computation.30 | convolution fusion | flops 201326592 | bytes 2621440 | tf_op jit(solution)/shard_map/transpose(jvp(hnjk,hnjv->nhkv))/dot_general | solution.py:46
  151.5 5.2 %all-to-all-start.6 = ((bf16[4,128,256]{1,2,0:T(8,128)(2,1)}), bf16[4,128,256]{1,2,0:T(8,128)(2,1)S(1)}, u32[]{:S(2)}, u32[]{:S(2)}) async-start(bf16[4,128,256]{1,2,0:T(8,128)(2,1)} %copy.226), calls=%async_computation.6 | async-start | bytes 524288 | tf_op jit(solution)/shard_map/all_to_all | solution.py:104
  159.6 25.8 %fusion.47 = f32[4,8,64,64]{3,1,2,0:T(8,128)S(1)} fusion(f32[4,8,64,64]{3,1,2,0:T(8,128)S(1)} %copy.246), kind=kOutput, calls=%fused_computation.85 | output fusion | flops 8257536 | bytes 1048576 | tf_op jit(solution)/shard_map/transpose(jvp(jit(cumsum)))/reduce_window_sum | solution.py:34
  186.1 5.2 %all-to-all-start.7 = ((bf16[4,128,512]{2,1,0:T(8,128)(2,1)}), bf16[4,128,512]{2,1,0:T(8,128)(2,1)S(1)}, u32[]{:S(2)}, u32[]{:S(2)}) async-start(bf16[4,128,512]{2,1,0:T(8,128)(2,1)} %convert_element_type.84), calls=%async_computation.7 | async-start | bytes 1048576 | tf_op jit(solution)/shard_map/all_to_all | solution.py:107
  193.9 56.5 %all-reduce.3.cloned.1.call-done = f32[64,256]{1,0:T(8,128)} async-done(((f32[64,256]{1,0:T(8,128)}), f32[64,256]{1,0:T(8,128)}) %all-reduce.3.cloned.1.call-update) | async-done | bytes 65552 | tf_op jit(solution)/shard_map/psum | solution.py:122
  250.4 14.1 %all_gather.7 = f32[64,1024]{1,0:T(8,128)S(1)} all-gather(f32[64,256]{1,0:T(8,128)} %all-reduce.3.cloned.1.call-done), channel_id=1, replica_groups=mesh['sp'=4,'dp'=8] {'sp'}, dimensions={1}, use_global_device_ids=true | all-gather | bytes 327680 | tf_op jit(solution)/shard_map/all_gather | solution.py:123
  (132 shorter events, 37.8 us)
Async XLA Ops:
  8.0 41.7 %copy-start = (bf16[64,1024]{1,0:T(8,128)(2,1)S(1)}, bf16[64,1024]{1,0:T(8,128)(2,1)}, u32[]{:S(2)}) copy-start(bf16[64,1024]{1,0:T(8,128)(2,1)} %param.13) | copy-start | bytes 393220
  8.0 12.1 %all-to-all-start.1 = ((bf16[128,4,4]{0,2,1:T(4,128)(2,1)}), bf16[128,4,4]{0,2,1:T(4,128)(2,1)S(1)}, u32[]{:S(2)}, u32[]{:S(2)}) async-start(bf16[128,4,4]{0,2,1:T(4,128)(2,1)} %bitcast.169), calls=%async_computation.1 | async-start | bytes 8192 | tf_op jit(solution)/shard_map/all_to_all | solution.py:75
  20.1 3.6 %copy-start.20 = (bf16[128,1024]{1,0:T(8,128)(2,1)S(1)}, bf16[128,1024]{1,0:T(8,128)(2,1)}, u32[]{:S(2)}) copy-start(bf16[128,1024]{1,0:T(8,128)(2,1)} %param.9) | copy-start | bytes 786436
  20.1 11.4 %all-to-all-start.5 = ((bf16[128,4,256]{0,2,1:T(8,128)(2,1)}), bf16[128,4,256]{0,2,1:T(8,128)(2,1)S(1)}, u32[]{:S(2)}, u32[]{:S(2)}) async-start(bf16[128,4,256]{0,2,1:T(8,128)(2,1)} %bitcast.24), calls=%async_computation.5 | async-start | bytes 524288 | tf_op jit(solution)/shard_map/all_to_all | solution.py:71
  23.6 11.3 %copy-start.17 = (bf16[128,2048]{1,0:T(8,128)(2,1)S(1)}, bf16[128,2048]{1,0:T(8,128)(2,1)}, u32[]{:S(2)}) copy-start(bf16[128,2048]{1,0:T(8,128)(2,1)} %param.11) | copy-start | bytes 1572868
  31.5 19.5 %all-to-all-start = ((bf16[128,4,256]{0,2,1:T(8,128)(2,1)}), bf16[128,4,256]{0,2,1:T(8,128)(2,1)S(1)}, u32[]{:S(2)}, u32[]{:S(2)}) async-start(bf16[128,4,256]{0,2,1:T(8,128)(2,1)} %bitcast), calls=%async_computation | async-start | bytes 524288 | tf_op jit(solution)/shard_map/all_to_all | solution.py:72
  35.0 1.6 copy-start.31
  49.0 1.9 copy-start.21
  51.0 5.4 %copy-start.18 = (bf16[128,2048]{1,0:T(8,128)(2,1)S(1)}, bf16[128,2048]{1,0:T(8,128)(2,1)}, u32[]{:S(2)}) copy-start(bf16[128,2048]{1,0:T(8,128)(2,1)} %param.10) | copy-start | bytes 1572868
  51.7 32.2 %all-to-all-start.3 = ((bf16[128,4,512]{2,0,1:T(8,128)(2,1)}), bf16[128,4,512]{2,0,1:T(8,128)(2,1)}, u32[]{:S(2)}, u32[]{:S(2)}) async-start(bf16[128,4,512]{2,0,1:T(8,128)(2,1)} %bitcast.143), calls=%async_computation.3 | async-start | bytes 1048576 | tf_op jit(solution)/shard_map/all_to_all | solution.py:74
  83.9 15.5 %all-to-all-start.2 = ((bf16[128,4,512]{2,0,1:T(8,128)(2,1)}), bf16[128,4,512]{2,0,1:T(8,128)(2,1)}, u32[]{:S(2)}, u32[]{:S(2)}) async-start(bf16[128,4,512]{2,0,1:T(8,128)(2,1)} %bitcast.144), calls=%async_computation.2 | async-start | bytes 1048576 | tf_op jit(solution)/shard_map/all_to_all | solution.py:73
  102.5 7.0 %copy-start.5 = (bf16[4,512,128]{2,1,0:T(8,128)(2,1)}, bf16[4,512,128]{2,1,0:T(8,128)(2,1)S(1)}, u32[]{:S(2)}) copy-start(bf16[4,512,128]{2,1,0:T(8,128)(2,1)S(1)} %copy.198) | copy-start | bytes 1572868
  106.6 2.9 %copy-start.9 = (f32[8,4,64,128]{3,0,2,1:T(8,128)}, f32[8,4,64,128]{3,0,2,1:T(8,128)S(1)}, u32[]{:S(2)}) copy-start(f32[8,4,64,128]{3,0,2,1:T(8,128)S(1)} %convolution_bitcast_fusion) | copy-start | bytes 3145732
  117.3 2.0 copy-start.26
  122.2 1.4 copy-start.29
  123.6 1.4 copy-start.27
  126.7 1.3 copy-start.11
  126.7 1.5 copy-start.12
  126.7 1.8 copy-start.13
  128.5 1.5 copy-start.8
  128.5 1.5 copy-start.10
  138.8 4.8 %copy-start.28 = (pred[64,64]{1,0:T(8,128)(4,1)S(1)}, pred[64,64]{1,0:T(8,128)(4,1)}, u32[]{:S(2)}) copy-start(pred[64,64]{1,0:T(8,128)(4,1)} %iota_compare_fusion) | copy-start | bytes 12292
  138.8 12.7 %all-to-all-start.4 = ((bf16[4,128,256]{1,2,0:T(8,128)(2,1)}), bf16[4,128,256]{1,2,0:T(8,128)(2,1)S(1)}, u32[]{:S(2)}, u32[]{:S(2)}) async-start(bf16[4,128,256]{1,2,0:T(8,128)(2,1)} %copy.213), calls=%async_computation.4 | async-start | bytes 524288 | tf_op jit(solution)/shard_map/all_to_all | solution.py:101
  143.6 3.1 %copy-start.14 = (bf16[4,8,64,64]{2,3,1,0:T(8,128)(2,1)S(1)}, bf16[4,8,64,64]{2,3,1,0:T(8,128)(2,1)}, u32[]{:S(2)}) copy-start(bf16[4,8,64,64]{2,3,1,0:T(8,128)(2,1)} %get-tuple-element.23) | copy-start | bytes 786436
  148.3 8.4 %copy-start.6 = (f32[4,8,64,64]{3,2,1,0:T(8,128)S(1)}, f32[4,8,64,64]{3,2,1,0:T(8,128)}, u32[]{:S(2)}) copy-start(f32[4,8,64,64]{3,2,1,0:T(8,128)} %convolution_select_fusion.2) | copy-start | bytes 1572868
  151.5 5.3 %copy-start.2 = (bf16[4,512,128]{2,1,0:T(8,128)(2,1)S(1)}, bf16[4,512,128]{2,1,0:T(8,128)(2,1)}, u32[]{:S(2)}) copy-start(bf16[4,512,128]{2,1,0:T(8,128)(2,1)} %copy.205) | copy-start | bytes 1572868
  151.5 34.6 %all-to-all-start.6 = ((bf16[4,128,256]{1,2,0:T(8,128)(2,1)}), bf16[4,128,256]{1,2,0:T(8,128)(2,1)S(1)}, u32[]{:S(2)}, u32[]{:S(2)}) async-start(bf16[4,128,256]{1,2,0:T(8,128)(2,1)} %copy.226), calls=%async_computation.6 | async-start | bytes 524288 | tf_op jit(solution)/shard_map/all_to_all | solution.py:104
  157.7 1.4 copy-start.7
  186.1 5.3 %copy-start.19 = (f32[256,512]{1,0:T(8,128)S(1)}, f32[256,512]{1,0:T(8,128)}, u32[]{:S(2)}) copy-start(f32[256,512]{1,0:T(8,128)} %get-tuple-element.30) | copy-start | bytes 1572868
  186.1 81.5 %all-to-all-start.7 = ((bf16[4,128,512]{2,1,0:T(8,128)(2,1)}), bf16[4,128,512]{2,1,0:T(8,128)(2,1)S(1)}, u32[]{:S(2)}, u32[]{:S(2)}) async-start(bf16[4,128,512]{2,1,0:T(8,128)(2,1)} %convert_element_type.84), calls=%async_computation.7 | async-start | bytes 1048576 | tf_op jit(solution)/shard_map/all_to_all | solution.py:107
  191.3 59.1 %all-reduce.3.cloned.1.call-start = ((), (), s32[]{:S(2)}) async-start(), calls=%async_computation.10 | async-start | bytes 131072 | tf_op jit(solution)/shard_map/psum | solution.py:122
  193.0 71.5 %reduce-scatter.2.cloned.1.call-start = ((), (), s32[]{:S(2)}) async-start(), calls=%async_computation.9 | async-start | bytes 163840 | tf_op jit(solution)/shard_map/reduce_scatter | solution.py:116
  (11 other events, 10.9 us)
Sparse Core Ops, SparseCore 0:
  195.7 54.6 all-reduce.2
Sparse Core Ops, SparseCore 1:
  196.3 20.9 reduce-scatter.1
where the time goes:
time: 279 us; the launch traced here: 277 us
  waiting for transfers between devices  67.7 us (24%)
  other arithmetic  56 us (20%)
  local copies, waits for them, and re-layouts  39.8 us (14%)
  starting transfers between devices  38 us (14%)
  matrix products  32.9 us (12%)
  blocking collectives  26.6 us (10%)
  between operations  15.9 us (6%)
    psum x1, waiting for transfers between devices, on_device(): summed = lax.psum(local_weight, 'dp')  56.5 us
    another operation x2, other arithmetic, gla_forward(): cumulative = jnp.cumsum(blocked(logarithm_decay), axis=2)  51.6 us
    all_gather x1, blocking collectives, on_device(): weight_grad = lax.all_gather(summed, 'sp', axis=1, tiled=True)  14.1 us
    all_gather x1, blocking collectives, on_device(): hidden_code_rows = lax.all_gather(compact_factor, 'sp', axis=0, tiled=True)  12.5 us
    unnamed x72, local copies, waits for them, and re-layouts  10.3 us
    dot_general x3, matrix products, carry_states(): return jnp.einsum('hnmk,mhkv->nhkv', weights, increments, precision=highest)  9.75 us
    dot_general x3, matrix products, gla_forward(): jnp.einsum('hnik,hnjk->hnij', query_decayed, key_inverse, precision=highest)  8.12 us
    all_to_all x1, waiting for transfers between devices, on_device(): lax.all_to_all(probe_vectors, 'sp', split_axis=1, concat_axis=0, tiled=True)  7.02 us
  transfers between devices with their start and end apart: 10, of which 4 were waited for; matrix products, arithmetic and copies ran while one was open for 31% of the time, Pallas kernels for 0%

commit v1 on v0

--- a/solution.py
+++ b/solution.py
@@ -119,7 +119,7 @@
     local_weight = jnp.einsum(
         "sr,sc->rc", hidden_code_rows, gate_grad, preferred_element_type=jnp.float32
     )
-    summed = lax.psum(local_weight, "dp")
+    summed = jnp.sum(lax.all_gather(local_weight, axis_name="dp"), axis=0)
     weight_grad = lax.all_gather(summed, "sp", axis=1, tiled=True)
     return (query_grad, key_grad, value_grad, latent_grad, weight_grad)
 

time: 279 us -> 231 us (0.83)
  waiting for transfers between devices: 67.7 us -> 11.2 us
  blocking collectives: 26.6 us -> 37 us
    psum x1 -> x0, waiting for transfers between devices: 56.5 us -> none  [on_device(): summed = lax.psum(local_weight, 'dp')]
    all_gather x0 -> x1, blocking collectives: none -> 9.86 us  [on_device(): summed = jnp.sum(lax.all_gather(local_weight, axis_name='dp'), axis=0)]
  transfers between devices with their start and end apart: 10 -> 9, of which waited for: 4 -> 3; matrix products, arithmetic and copies ran while one was open for 31% -> 37% of each run, Pallas kernels for 0% -> 0%
where the time goes in v1:
time: 231 us; the launch traced here: 229 us
  other arithmetic  56 us (24%)
  local copies, waits for them, and re-layouts  40 us (17%)
  starting transfers between devices  38 us (16%)
  blocking collectives  37 us (16%)
  matrix products  32.3 us (14%)
  between operations  14.5 us (6%)
  waiting for transfers between devices  11.2 us (5%)
    another operation x2, other arithmetic, gla_forward(): cumulative = jnp.cumsum(blocked(logarithm_decay), axis=2)  51.6 us
    all_gather x1, blocking collectives, on_device(): weight_grad = lax.all_gather(summed, 'sp', axis=1, tiled=True)  14.7 us
    all_gather x1, blocking collectives, on_device(): hidden_code_rows = lax.all_gather(compact_factor, 'sp', axis=0, tiled=True)  12.5 us
    unnamed x72, local copies, waits for them, and re-layouts  10.4 us
    all_gather x1, blocking collectives, on_device(): summed = jnp.sum(lax.all_gather(local_weight, axis_name='dp'), axis=0)  9.86 us
    dot_general x3, matrix products, carry_states(): return jnp.einsum('hnmk,mhkv->nhkv', weights, increments, precision=highest)  9.76 us
    dot_general x3, matrix products, gla_forward(): jnp.einsum('hnik,hnjk->hnij', query_decayed, key_inverse, precision=highest)  8.14 us
    all_to_all x1, waiting for transfers between devices, on_device(): lax.all_to_all(probe_vectors, 'sp', split_axis=1, concat_axis=0, tiled=True)  7.02 us
  transfers between devices with their start and end apart: 9, of which 3 were waited for; matrix products, arithmetic and copies ran while one was open for 37% of the time, Pallas kernels for 0%

profile of v1, /device:TPU:0, one launch (start us, length us, event | category | flops | bytes accessed | tf_op | source)
XLA Modules:
  0.0 229.0 jit_solution(18394739539287099076)
XLA Ops:
  7.2 6.5 %all-to-all-start.1 = ((bf16[128,4,4]{0,2,1:T(4,128)(2,1)}), bf16[128,4,4]{0,2,1:T(4,128)(2,1)S(1)}, u32[]{:S(2)}, u32[]{:S(2)}) async-start(bf16[128,4,4]{0,2,1:T(4,128)(2,1)} %bitcast.171), calls=%async_computation.1 | async-start | bytes 8192 | tf_op jit(solution)/shard_map/all_to_all | solution.py:75
  13.7 1.8 copy.214
  15.5 3.8 %all-to-all-done.1 = bf16[128,4,4]{0,2,1:T(4,128)(2,1)S(1)} async-done(((bf16[128,4,4]{0,2,1:T(4,128)(2,1)}), bf16[128,4,4]{0,2,1:T(4,128)(2,1)S(1)}, u32[]{:S(2)}, u32[]{:S(2)}) %all-to-all-start.1) | async-done | bytes 4128 | tf_op jit(solution)/shard_map/all_to_all | solution.py:75
  19.3 3.5 %all-to-all-start.5 = ((bf16[128,4,256]{0,2,1:T(8,128)(2,1)}), bf16[128,4,256]{0,2,1:T(8,128)(2,1)S(1)}, u32[]{:S(2)}, u32[]{:S(2)}) async-start(bf16[128,4,256]{0,2,1:T(8,128)(2,1)} %bitcast.24), calls=%async_computation.5 | async-start | bytes 524288 | tf_op jit(solution)/shard_map/all_to_all | solution.py:71
  23.7 7.0 %all-to-all-done.5 = bf16[128,4,256]{0,2,1:T(8,128)(2,1)S(1)} async-done(((bf16[128,4,256]{0,2,1:T(8,128)(2,1)}), bf16[128,4,256]{0,2,1:T(8,128)(2,1)S(1)}, u32[]{:S(2)}, u32[]{:S(2)}) %all-to-all-start.5) | async-done | bytes 262176 | tf_op jit(solution)/shard_map/all_to_all | solution.py:71
  30.7 3.4 %all-to-all-start = ((bf16[128,4,256]{0,2,1:T(8,128)(2,1)}), bf16[128,4,256]{0,2,1:T(8,128)(2,1)S(1)}, u32[]{:S(2)}, u32[]{:S(2)}) async-start(bf16[128,4,256]{0,2,1:T(8,128)(2,1)} %bitcast), calls=%async_computation | async-start | bytes 524288 | tf_op jit(solution)/shard_map/all_to_all | solution.py:72
  35.8 12.5 %all_gather.12 = bf16[512,64]{0,1:T(8,128)(2,1)S(1)} all-gather(bf16[128,64]{0,1:T(8,128)(2,1)S(1)} %copy-done.31), channel_id=1, replica_groups=mesh['sp'=4,'dp'=8] {'sp'}, dimensions={0}, use_global_device_ids=true | all-gather | bytes 81920 | tf_op jit(solution)/shard_map/all_gather | solution.py:78
  50.9 4.1 %all-to-all-start.3 = ((bf16[128,4,512]{2,0,1:T(8,128)(2,1)}), bf16[128,4,512]{2,0,1:T(8,128)(2,1)}, u32[]{:S(2)}, u32[]{:S(2)}) async-start(bf16[128,4,512]{2,0,1:T(8,128)(2,1)} %bitcast.144), calls=%async_computation.3 | async-start | bytes 1048576 | tf_op jit(solution)/shard_map/all_to_all | solution.py:74
  57.2 25.9 %fusion.46 = f32[4,8,64,64]{3,1,2,0:T(8,128)S(1)} fusion(f32[4,8,64,64]{3,1,2,0:T(8,128)S(1)} %copy.194), kind=kOutput, calls=%fused_computation.84 | output fusion | flops 8257536 | bytes 1048576 | tf_op jit(solution)/shard_map/jvp(jit(cumsum))/reduce_window_sum | solution.py:34
  83.1 5.1 %all-to-all-start.2 = ((bf16[128,4,512]{2,0,1:T(8,128)(2,1)}), bf16[128,4,512]{2,0,1:T(8,128)(2,1)}, u32[]{:S(2)}, u32[]{:S(2)}) async-start(bf16[128,4,512]{2,0,1:T(8,128)(2,1)} %bitcast.145), calls=%async_computation.2 | async-start | bytes 1048576 | tf_op jit(solution)/shard_map/all_to_all | solution.py:73
  94.3 2.0 reshape.161
  96.2 1.9 copy.205
  98.5 2.0 reshape.159
  102.9 2.9 %convolution_bitcast_fusion = f32[8,4,64,128]{3,0,2,1:T(8,128)S(1)} fusion(f32[4,64,128,8]{2,1,3,0:T(8,128)S(1)} %convolution_bitcast_fusion.3, f32[4,8,64]{1,2,0:T(8,128)S(1)} %copy-done.23, f32[4,8,64]{1,2,0:T(8,128)S(1)} %copy-done.24, pred[8,8]{1,0:T(8,128)(4,1)S(1)} %copy-done.32), kind=kOutput, calls=%fused_computation.4 | convolution fusion | flops 25214976 | bytes 2113600 | tf_op jit(solution)/shard_map/transpose(jvp(hnmk,mhkv->nhkv))/dot_general | solution.py:23
  105.8 2.8 %fusion.18 = (f32[4,8,64]{2,1,0:T(8,128)}, f32[4,8,64,64]{2,3,1,0:T(8,128)S(1)}, f32[4,8,64,64]{2,3,1,0:T(8,128)}) fusion(f32[4,8,64,64]{2,3,1,0:T(8,128)S(1)} %copy.195, f32[4,8,64,64]{2,1,3,0:T(8,128)S(1)} %reshape.166, f32[4,8,64]{2,1,0:T(8,128)S(1)} %slice_bitcast_fusion, bf16[4,8,64,128]{3,2,1,0:T(8,128)(2,1)S(1)} %bitcast.151, ...), kind=kOutput, calls=%fused_computation.40 | convolution fusion | flops 201979904 | bytes 3686400 | tf_op jit(solution)/shard_map/transpose(jvp(hnjk,hnjv->nhkv))/dot_general | solution.py:46
  109.6 2.5 %convolution_bitcast_fusion.1 = f32[8,4,64,128]{3,0,2,1:T(8,128)S(1)} fusion(f32[8,4,64,128]{3,2,1,0:T(8,128)S(1)} %fusion.6, f32[4,8,64]{1,2,0:T(8,128)S(1)} %copy-done.23, f32[4,8,64]{1,2,0:T(8,128)S(1)} %copy-done.24, pred[8,8]{1,0:T(8,128)(4,1)S(1)} %copy-done.32), kind=kOutput, calls=%fused_computation.6 | convolution fusion | flops 25214976 | bytes 2113600 | tf_op jit(solution)/shard_map/jvp(hnmk,mhkv->nhkv)/dot_general | solution.py:23
  112.1 4.3 %fusion.45 = (f32[4,8,64]{1,2,0:T(8,128)}, f32[4,8,64]{1,2,0:T(8,128)}) fusion(f32[4,8,64]{1,2,0:T(8,128)S(1)} %copy-done.23, f32[4,8,64]{1,2,0:T(8,128)S(1)} %copy-done.24, f32[8,4,64,128]{3,2,1,0:T(8,128)S(1)} %fusion.6, f32[4,64,128,8]{2,1,3,0:T(8,128)S(1)} %convolution_bitcast_fusion.3, pred[8,8]{1,0:T(8,128)(4,1)S(1)} %copy-done.32), kind=kOutput, calls=%fused_computation.83 | convolution fusion | flops 25276416 | bytes 2129984 | tf_op jit(solution)/shard_map/transpose(jvp(hnmk,mhkv->nhkv))/dot_general | solution.py:23
  116.4 2.0 convolution_bitcast_fusion.4
  121.4 1.4 copy.244
  122.8 1.4 copy.245
  124.2 1.6 convolution_select_fusion
  127.7 1.5 fusion.3
  129.2 3.7 %pad_add_fusion = (f32[4,8,64,64]{2,3,1,0:T(8,128)}, bf16[4,8,64,64]{2,3,1,0:T(8,128)(2,1)}, bf16[4,8,64,64]{2,3,1,0:T(8,128)(2,1)S(1)}) fusion(f32[4,8,1,64]{2,3,1,0:T(8,128)S(1)} %fusion.3, f32[4,8,64,64]{2,3,1,0:T(8,128)S(1)} %fusion.44, f32[4,8,64,64]{2,1,3,0:T(8,128)S(1)} %mul.72, f32[4,8,64,64]{2,3,1,0:T(8,128)S(1)} %copy.195, ...), kind=kOutput, calls=%fused_computation.22 | convolution fusion | flops 103677952 | bytes 4734976 | tf_op jit(solution)/shard_map/transpose(jvp(hnik,hnjk->hnij))/dot_general | solution.py:41
  136.3 1.7 copy.213
  137.9 4.8 %all-to-all-start.4 = ((bf16[4,128,256]{1,2,0:T(8,128)(2,1)}), bf16[4,128,256]{1,2,0:T(8,128)(2,1)S(1)}, u32[]{:S(2)}, u32[]{:S(2)}) async-start(bf16[4,128,256]{1,2,0:T(8,128)(2,1)} %copy.213), calls=%async_computation.4 | async-start | bytes 524288 | tf_op jit(solution)/shard_map/all_to_all | solution.py:101
  142.8 3.1 %convolution_select_fusion.2 = f32[4,8,64,64]{3,2,1,0:T(8,128)} fusion(pred[64,64]{1,0:T(8,128)(4,1)S(1)} %copy-done.28, f32[4,8,64,64]{2,1,3,0:T(8,128)S(1)} %reshape.166, f32[4,8,64,64]{2,3,1,0:T(8,128)S(1)} %copy.195, f32[4,8,64,64]{2,1,3,0:T(8,128)S(1)} %mul.72), kind=kOutput, calls=%fused_computation.11 | convolution fusion | flops 101187584 | bytes 2101248 | tf_op jit(solution)/shard_map/jvp(hnik,hnjk->hnij)/dot_general | solution.py:41
  147.5 3.2 %fusion.11 = f32[4,8,64,128]{3,2,1,0:T(8,128)S(1)} fusion(f32[4,8,64,64]{2,3,1,0:T(8,128)S(1)} %copy-done.4, f32[8,4,64,128]{3,0,2,1:T(8,128)} %copy-done.9), kind=kOutput, calls=%fused_computation.30 | convolution fusion | flops 201326592 | bytes 2621440 | tf_op jit(solution)/shard_map/transpose(jvp(hnjk,hnjv->nhkv))/dot_general | solution.py:46
  150.7 5.2 %all-to-all-start.6 = ((bf16[4,128,256]{1,2,0:T(8,128)(2,1)}), bf16[4,128,256]{1,2,0:T(8,128)(2,1)S(1)}, u32[]{:S(2)}, u32[]{:S(2)}) async-start(bf16[4,128,256]{1,2,0:T(8,128)(2,1)} %copy.226), calls=%async_computation.6 | async-start | bytes 524288 | tf_op jit(solution)/shard_map/all_to_all | solution.py:104
  158.8 25.8 %fusion.47 = f32[4,8,64,64]{3,1,2,0:T(8,128)S(1)} fusion(f32[4,8,64,64]{3,1,2,0:T(8,128)S(1)} %copy.246), kind=kOutput, calls=%fused_computation.85 | output fusion | flops 8257536 | bytes 1048576 | tf_op jit(solution)/shard_map/transpose(jvp(jit(cumsum)))/reduce_window_sum | solution.py:34
  185.3 5.2 %all-to-all-start.7 = ((bf16[4,128,512]{2,1,0:T(8,128)(2,1)}), bf16[4,128,512]{2,1,0:T(8,128)(2,1)S(1)}, u32[]{:S(2)}, u32[]{:S(2)}) async-start(bf16[4,128,512]{2,1,0:T(8,128)(2,1)} %convert_element_type.84), calls=%async_computation.7 | async-start | bytes 1048576 | tf_op jit(solution)/shard_map/all_to_all | solution.py:107
  192.6 9.9 %all-gather = f32[512,256]{1,0:T(8,128)S(1)} all-gather(f32[64,256]{1,0:T(8,128)S(1)} %convolution_bitcast_fusion.5), channel_id=2, replica_groups=mesh['sp'=4,'dp'=8] {'dp'}, dimensions={0}, use_global_device_ids=true | all-gather | bytes 589824 | tf_op jit(solution)/shard_map/all_gather | solution.py:122
  202.4 14.7 %all_gather.15 = f32[64,1024]{1,0:T(8,128)S(1)} all-gather(f32[64,256]{1,0:T(8,128)S(1)} %reduce_sum.50), channel_id=1, replica_groups=mesh['sp'=4,'dp'=8] {'sp'}, dimensions={1}, use_global_device_ids=true | all-gather | bytes 327680 | tf_op jit(solution)/shard_map/all_gather | solution.py:123
  (131 shorter events, 37.3 us)
Async XLA Ops:
  7.2 41.7 %copy-start = (bf16[64,1024]{1,0:T(8,128)(2,1)S(1)}, bf16[64,1024]{1,0:T(8,128)(2,1)}, u32[]{:S(2)}) copy-start(bf16[64,1024]{1,0:T(8,128)(2,1)} %param.13) | copy-start | bytes 393220
  7.2 12.1 %all-to-all-start.1 = ((bf16[128,4,4]{0,2,1:T(4,128)(2,1)}), bf16[128,4,4]{0,2,1:T(4,128)(2,1)S(1)}, u32[]{:S(2)}, u32[]{:S(2)}) async-start(bf16[128,4,4]{0,2,1:T(4,128)(2,1)} %bitcast.171), calls=%async_computation.1 | async-start | bytes 8192 | tf_op jit(solution)/shard_map/all_to_all | solution.py:75
  19.3 3.6 %copy-start.20 = (bf16[128,1024]{1,0:T(8,128)(2,1)S(1)}, bf16[128,1024]{1,0:T(8,128)(2,1)}, u32[]{:S(2)}) copy-start(bf16[128,1024]{1,0:T(8,128)(2,1)} %param.9) | copy-start | bytes 786436
  19.3 11.4 %all-to-all-start.5 = ((bf16[128,4,256]{0,2,1:T(8,128)(2,1)}), bf16[128,4,256]{0,2,1:T(8,128)(2,1)S(1)}, u32[]{:S(2)}, u32[]{:S(2)}) async-start(bf16[128,4,256]{0,2,1:T(8,128)(2,1)} %bitcast.24), calls=%async_computation.5 | async-start | bytes 524288 | tf_op jit(solution)/shard_map/all_to_all | solution.py:71
  22.8 11.3 %copy-start.17 = (bf16[128,2048]{1,0:T(8,128)(2,1)S(1)}, bf16[128,2048]{1,0:T(8,128)(2,1)}, u32[]{:S(2)}) copy-start(bf16[128,2048]{1,0:T(8,128)(2,1)} %param.11) | copy-start | bytes 1572868
  30.7 19.5 %all-to-all-start = ((bf16[128,4,256]{0,2,1:T(8,128)(2,1)}), bf16[128,4,256]{0,2,1:T(8,128)(2,1)S(1)}, u32[]{:S(2)}, u32[]{:S(2)}) async-start(bf16[128,4,256]{0,2,1:T(8,128)(2,1)} %bitcast), calls=%async_computation | async-start | bytes 524288 | tf_op jit(solution)/shard_map/all_to_all | solution.py:72
  34.1 1.6 copy-start.31
  48.3 1.9 copy-start.21
  50.2 5.4 %copy-start.18 = (bf16[128,2048]{1,0:T(8,128)(2,1)S(1)}, bf16[128,2048]{1,0:T(8,128)(2,1)}, u32[]{:S(2)}) copy-start(bf16[128,2048]{1,0:T(8,128)(2,1)} %param.10) | copy-start | bytes 1572868
  50.9 32.2 %all-to-all-start.3 = ((bf16[128,4,512]{2,0,1:T(8,128)(2,1)}), bf16[128,4,512]{2,0,1:T(8,128)(2,1)}, u32[]{:S(2)}, u32[]{:S(2)}) async-start(bf16[128,4,512]{2,0,1:T(8,128)(2,1)} %bitcast.144), calls=%async_computation.3 | async-start | bytes 1048576 | tf_op jit(solution)/shard_map/all_to_all | solution.py:74
  83.1 15.5 %all-to-all-start.2 = ((bf16[128,4,512]{2,0,1:T(8,128)(2,1)}), bf16[128,4,512]{2,0,1:T(8,128)(2,1)}, u32[]{:S(2)}, u32[]{:S(2)}) async-start(bf16[128,4,512]{2,0,1:T(8,128)(2,1)} %bitcast.145), calls=%async_computation.2 | async-start | bytes 1048576 | tf_op jit(solution)/shard_map/all_to_all | solution.py:73
  101.7 7.0 %copy-start.5 = (bf16[4,512,128]{2,1,0:T(8,128)(2,1)}, bf16[4,512,128]{2,1,0:T(8,128)(2,1)S(1)}, u32[]{:S(2)}) copy-start(bf16[4,512,128]{2,1,0:T(8,128)(2,1)S(1)} %copy.198) | copy-start | bytes 1572868
  105.8 2.9 %copy-start.9 = (f32[8,4,64,128]{3,0,2,1:T(8,128)}, f32[8,4,64,128]{3,0,2,1:T(8,128)S(1)}, u32[]{:S(2)}) copy-start(f32[8,4,64,128]{3,0,2,1:T(8,128)S(1)} %convolution_bitcast_fusion) | copy-start | bytes 3145732
  116.4 2.0 copy-start.26
  121.4 1.4 copy-start.29
  122.8 1.4 copy-start.27
  125.8 1.3 copy-start.11
  125.8 1.5 copy-start.12
  125.8 1.8 copy-start.13
  127.7 1.5 copy-start.8
  127.7 1.5 copy-start.10
  137.9 4.9 %copy-start.28 = (pred[64,64]{1,0:T(8,128)(4,1)S(1)}, pred[64,64]{1,0:T(8,128)(4,1)}, u32[]{:S(2)}) copy-start(pred[64,64]{1,0:T(8,128)(4,1)} %iota_compare_fusion) | copy-start | bytes 12292
  137.9 12.7 %all-to-all-start.4 = ((bf16[4,128,256]{1,2,0:T(8,128)(2,1)}), bf16[4,128,256]{1,2,0:T(8,128)(2,1)S(1)}, u32[]{:S(2)}, u32[]{:S(2)}) async-start(bf16[4,128,256]{1,2,0:T(8,128)(2,1)} %copy.213), calls=%async_computation.4 | async-start | bytes 524288 | tf_op jit(solution)/shard_map/all_to_all | solution.py:101
  142.8 3.1 %copy-start.14 = (bf16[4,8,64,64]{2,3,1,0:T(8,128)(2,1)S(1)}, bf16[4,8,64,64]{2,3,1,0:T(8,128)(2,1)}, u32[]{:S(2)}) copy-start(bf16[4,8,64,64]{2,3,1,0:T(8,128)(2,1)} %get-tuple-element.23) | copy-start | bytes 786436
  146.3 1.2 copy-start.4
  147.5 8.4 %copy-start.6 = (f32[4,8,64,64]{3,2,1,0:T(8,128)S(1)}, f32[4,8,64,64]{3,2,1,0:T(8,128)}, u32[]{:S(2)}) copy-start(f32[4,8,64,64]{3,2,1,0:T(8,128)} %convolution_select_fusion.2) | copy-start | bytes 1572868
  150.7 5.3 %copy-start.2 = (bf16[4,512,128]{2,1,0:T(8,128)(2,1)S(1)}, bf16[4,512,128]{2,1,0:T(8,128)(2,1)}, u32[]{:S(2)}) copy-start(bf16[4,512,128]{2,1,0:T(8,128)(2,1)} %copy.205) | copy-start | bytes 1572868
  150.7 34.6 %all-to-all-start.6 = ((bf16[4,128,256]{1,2,0:T(8,128)(2,1)}), bf16[4,128,256]{1,2,0:T(8,128)(2,1)S(1)}, u32[]{:S(2)}, u32[]{:S(2)}) async-start(bf16[4,128,256]{1,2,0:T(8,128)(2,1)} %copy.226), calls=%async_computation.6 | async-start | bytes 524288 | tf_op jit(solution)/shard_map/all_to_all | solution.py:104
  156.9 1.4 copy-start.7
  185.3 5.3 %copy-start.19 = (f32[256,512]{1,0:T(8,128)S(1)}, f32[256,512]{1,0:T(8,128)}, u32[]{:S(2)}) copy-start(f32[256,512]{1,0:T(8,128)} %get-tuple-element.30) | copy-start | bytes 1572868
  185.3 34.9 %all-to-all-start.7 = ((bf16[4,128,512]{2,1,0:T(8,128)(2,1)}), bf16[4,128,512]{2,1,0:T(8,128)(2,1)S(1)}, u32[]{:S(2)}, u32[]{:S(2)}) async-start(bf16[4,128,512]{2,1,0:T(8,128)(2,1)} %convert_element_type.84), calls=%async_computation.7 | async-start | bytes 1048576 | tf_op jit(solution)/shard_map/all_to_all | solution.py:107
  190.5 26.6 %reduce-scatter.2.cloned.1.call-start = ((), (), s32[]{:S(2)}) async-start(), calls=%async_computation.9 | async-start | bytes 163840 | tf_op jit(solution)/shard_map/reduce_scatter | solution.py:116
  (10 other events, 9.6 us)
Sparse Core Ops, SparseCore 0:
  194.1 21.3 reduce-scatter.1
